TPU v7x, 128 devices: a 2x2x16 block of a 8x8x16 slice. The times are simulated.
128 devices in a mesh: grp: 4 (over y, x), ep: 32 (over z, core).
Axes of the slice: x: 2, y: 2, z: 16, core: 2. Of those that a mesh axis runs over, the one named last changes fastest.
The devices are a block of a 8x8x16 slice.
Arguments:
- stream: bfloat16 [32768, 2048], P(('grp', 'ep')), parts along dimension 0, may hold values from -6 to 6
- norm_gain: float32 [2048], replicated, may hold values from 0.1 to 1.9
- routing: int32 [32768, 4], P(('grp', 'ep')), parts along dimension 0, may hold values from 0 to 63, all different within a row; in each aligned block of 256 rows (0 to 255, 256 to 511, ...) at most 32 rows name the same one
- gates: float32 [32768, 4], P(('grp', 'ep')), parts along dimension 0, may hold values from 0.1 to 1
- w_gate: bfloat16 [64, 2048, 512], P('ep'), may hold values from -0.125 to 0.125
- w_up: bfloat16 [64, 2048, 512], P('ep'), may hold values from -0.125 to 0.125
- w_down: bfloat16 [64, 512, 2048], P('ep'), may hold values from -0.25 to 0.25
- shared_gate: bfloat16 [2048, 512], replicated, may hold values from -0.125 to 0.125
- shared_up: bfloat16 [2048, 512], replicated, may hold values from -0.125 to 0.125
- shared_down: bfloat16 [512, 2048], replicated, may hold values from -0.25 to 0.25
Outputs:
- mixed: bfloat16 [32768, 2048], P(('grp', 'ep')), parts along dimension 0
There are 4 independent parts, one for each index of `grp`. A program takes and returns all parts, laid end to end along the dimension named above; an argument that names none is the same for every part. Nothing has to cross between parts.
Inputs may be any that keep to these rules, and one draw needn't show every extreme that they name: `routing`: each token names 4 different experts. Among the 256 tokens of one index of ep no expert is named more than 32 times, and on some index an expert is named exactly 32 times.
All inputs are finite; a program needn't handle non-finite values.
Results may differ from a plain program's by a relative error of at most 0.007.
Values may be sent and summed in bfloat16 or wider, within the bound.
No kernel may reach another device: no remote copies, remote signals or barrier semaphores. Data moves between devices by JAX's collectives and lax.ppermute only.
A program may use at most 128 MiB of HBM per device.

v0:
```python
import jax
import jax.numpy as jnp
from jax import lax
from jax.sharding import Mesh
from jax.sharding import PartitionSpec as P

EP = ("ep_0", "ep_1")
GRP_EP = ("grp", "ep_0", "ep_1")


def joined_along(tiles, dim):
    tiles = jnp.moveaxis(tiles, 0, dim)
    shape = tiles.shape
    return tiles.reshape(*shape[:dim], shape[dim] * shape[dim + 1], *shape[dim + 2 :])


def stacked_from(x, axes, sequence):
    tiles = x[None]
    for k in sequence:
        tiles = lax.all_gather(tiles, axes[k], axis=0, tiled=True)
    current = [lax.axis_size(axes[k]) for k in reversed(sequence)]
    tiles = tiles.reshape(*current, *x.shape)
    turned = sorted(range(len(sequence)), key=lambda place: sequence[len(sequence) - 1 - place])
    return tiles.transpose(*turned, *range(len(sequence), tiles.ndim)).reshape(-1, *x.shape)


def whole_of(x, axes, sequence, dim):
    return joined_along(stacked_from(x, axes, sequence), dim)


def layer_norm(stream, norm_gain):
    widened = stream.astype(jnp.float32)
    row_mean = jnp.mean(widened, axis=-1, keepdims=True)
    variance = jnp.mean(jnp.square(widened - row_mean), axis=-1, keepdims=True)
    return ((widened - row_mean) * lax.rsqrt(variance + 1e-05) * norm_gain).astype(jnp.bfloat16)


def shared_branch(normed, shared_gate, shared_up, shared_down):
    shared_hidden = (
        jax.nn.silu(jnp.dot(normed, shared_gate, preferred_element_type=jnp.float32))
        * jnp.dot(normed, shared_up, preferred_element_type=jnp.float32)
    ).astype(jnp.bfloat16)
    return jnp.dot(shared_hidden, shared_down, preferred_element_type=jnp.float32)


def serve_rows(received, w_gate, w_up, w_down):
    local_count = w_gate.shape[0]
    blocks = received.reshape((-1, local_count) + received.shape[1:])
    gate_act = jnp.einsum("sxcd,xdh->sxch", blocks, w_gate, preferred_element_type=jnp.float32)
    up_act = jnp.einsum("sxcd,xdh->sxch", blocks, w_up, preferred_element_type=jnp.float32)
    hidden = (jax.nn.silu(gate_act) * up_act).astype(jnp.bfloat16)
    produced = jnp.einsum(
        "sxch,xhd->sxcd", hidden, w_down, preferred_element_type=jnp.float32
    ).astype(jnp.bfloat16)
    return lax.all_to_all(
        produced.reshape(received.shape), EP, split_axis=0, concat_axis=0, tiled=True
    )


def on_device(
    stream, norm_gain, routing, gates, w_gate, w_up, w_down, shared_gate, shared_up, shared_down
):
    tok_rows, top_count = routing.shape
    local_count = w_gate.shape[0]
    peer_count = lax.axis_size(EP)
    experts = local_count * peer_count
    capacity = 2 * tok_rows * top_count // experts
    normed = layer_norm(stream, norm_gain)
    row_ids = jnp.arange(tok_rows, dtype=jnp.int32)
    lower = (row_ids[:, None] > row_ids[None, :]).astype(jnp.bfloat16)
    slot_ids = jnp.arange(capacity, dtype=jnp.int32).astype(jnp.float32)
    expert_hits = (
        routing[:, :, None] == jnp.arange(experts, dtype=jnp.int32)[None, None, :]
    ).astype(jnp.float32)
    token_hits = jnp.sum(expert_hits, axis=1).astype(jnp.bfloat16)
    earlier = jnp.dot(lower, token_hits, preferred_element_type=jnp.float32)
    slot_index = jnp.sum(earlier[:, None, :] * expert_hits, axis=2)
    slot_hits = (slot_index[:, :, None] == slot_ids[None, None, :]).astype(jnp.float32)
    gate_table = jnp.sum(
        gates[:, :, None, None] * expert_hits[:, :, :, None] * slot_hits[:, :, None, :], axis=1
    )
    all_normed = lax.all_gather(normed, EP, axis=0, tiled=True)
    all_routing = whole_of(routing, ("ep_0", "ep_1"), (0, 1), 0)
    first_expert = lax.axis_index(EP) * local_count
    shifted = all_routing.reshape(peer_count, tok_rows, top_count) - first_expert
    local_hits = (
        shifted[:, :, :, None] == jnp.arange(local_count, dtype=jnp.int32)[None, None, None, :]
    ).astype(jnp.float32)
    hits_here = jnp.sum(local_hits, axis=2).astype(jnp.bfloat16)
    prior_here = jnp.einsum("ab,pbx->pax", lower, hits_here, preferred_element_type=jnp.float32)
    placing_here = (
        hits_here.astype(jnp.float32)[:, :, :, None]
        * (prior_here[:, :, :, None] == slot_ids[None, None, None, :]).astype(jnp.float32)
    ).astype(jnp.bfloat16)
    sources = all_normed.reshape(peer_count, tok_rows, all_normed.shape[1])
    incoming = jnp.einsum(
        "ptxc,ptd->pxcd", placing_here, sources, preferred_element_type=jnp.float32
    ).astype(jnp.bfloat16)
    returned = serve_rows(
        incoming.reshape(peer_count * local_count, capacity, all_normed.shape[1]),
        w_gate,
        w_up,
        w_down,
    )
    weight_high = gate_table.astype(jnp.bfloat16)
    weight_low = (gate_table - weight_high.astype(jnp.float32)).astype(jnp.bfloat16)
    routed = jnp.einsum("tec,ecd->td", weight_high, returned, preferred_element_type=jnp.float32)
    routed = routed + jnp.einsum(
        "tec,ecd->td", weight_low, returned, preferred_element_type=jnp.float32
    )
    shared = shared_branch(normed, shared_gate, shared_up, shared_down)
    return (routed + shared).astype(jnp.bfloat16)


def solution(mesh):
    torus = Mesh(mesh.devices.reshape(mesh.shape["grp"], 16, 2), ("grp", "ep_0", "ep_1"))
    return jax.shard_map(
        on_device,
        mesh=torus,
        in_specs=(
            P(GRP_EP, None),
            P(),
            P(GRP_EP, None),
            P(GRP_EP, None),
            P(EP, None, None),
            P(EP, None, None),
            P(EP, None, None),
            P(),
            P(),
            P(),
        ),
        out_specs=P(GRP_EP, None),
        check_vma=False,
    )
```

profile of v0, /device:TPU:196, one launch (start us, length us, event | category | flops | bytes accessed | tf_op | source)
XLA Modules:
  0.0 663.4 jit_solution(12615390531225817600)
XLA Ops:
  6.5 0.0 copy-start
  6.6 0.0 copy-start.3
  6.6 0.0 all-gather.3.cloned.1.call-start
  6.6 1.6 convert_reduce_fusion
  8.2 1.6 fusion.23
  9.8 2.6 fusion.25
  12.4 0.1 all-gather.3.cloned.1.call-update
  12.5 0.0 copy-done.3
  12.5 37.3 %all-gather = s32[4096,4]{0,1:T(4,128)S(1)} all-gather(s32[256,4]{0,1:T(4,128)S(1)} %copy-done.3), channel_id=2, replica_groups=mesh['grp'=4,'ep_0'=16,'ep_1'=2] {'ep_0'}, dimensions={0}, use_global_device_ids=true | all-gather | bytes 69632 | tf_op jit(solution)/shard_map/all_gather | solution.py:20
  49.8 2.0 all_gather.10
  51.8 0.1 copy.45
  52.0 0.2 convolution_bitcast_fusion.2
  52.2 0.1 copy.47
  52.3 151.8 %all-gather.3.cloned.1.call-done = bf16[8192,2048]{1,0:T(8,128)(2,1)} async-done(((bf16[256,2048]{1,0:T(8,128)(2,1)}), bf16[8192,2048]{1,0:T(8,128)(2,1)}) %all-gather.3.cloned.1.call-update) | async-done | bytes 33554448 | tf_op jit(solution)/shard_map/all_gather | solution.py:82
  204.1 17.1 %convolution_convert_fusion = bf16[32,2,32,2048]{3,2,1,0:T(8,128)(2,1)} fusion(bf16[32,256,2048,1]{2,1,3,0:T(8,128)(2,1)} %bitcast.79, bf16[32,256,2]{1,2,0:T(2,128)(2,1)S(1)} %copy.48, f32[32,256,2]{1,2,0:T(2,128)S(1)} %copy.47, f32[32]{0:T(128)S(1)} %iota_convert_fusion), kind=kOutput, calls=%fused_computation.6 | convolution fusion | flops 2152726528 | bytes 42041472 | tf_op jit(solution)/shard_map/ptxc,ptd->pxcd/dot_general | solution.py:96
  221.2 11.0 %fusion.2 = f32[2,32,32,512]{3,2,1,0:T(8,128)} fusion(bf16[32,2,32,2048]{3,2,1,0:T(8,128)(2,1)} %convolution_convert_fusion, bf16[2,2048,512]{2,1,0:T(8,128)(2,1)} %param.14), kind=kOutput, calls=%fused_computation.4 | convolution fusion | flops 4294967296 | bytes 16777216 | tf_op jit(solution)/shard_map/sxcd,xdh->sxch/dot_general | solution.py:49
  232.2 15.3 %convert_bitcast_fusion = bf16[32,2,32,2048]{3,2,0,1:T(8,128)(2,1)} fusion(bf16[2,512,2048]{2,1,0:T(8,128)(2,1)} %param.16, f32[2,32,32,512]{3,2,1,0:T(8,128)} %fusion.2, bf16[2,2048,512]{2,1,0:T(8,128)(2,1)} %param.15, bf16[32,2,32,2048]{3,2,1,0:T(8,128)(2,1)} %convolution_convert_fusion), kind=kOutput, calls=%fused_computation | convolution fusion | flops 8600420352 | bytes 29360128 | tf_op jit(solution)/shard_map/sxch,xhd->sxcd/dot_general | solution.py:52
  247.5 8.3 %copy.51 = bf16[32,2,32,2048]{3,2,1,0:T(8,128)(2,1)} copy(bf16[32,2,32,2048]{3,2,0,1:T(8,128)(2,1)} %convert_bitcast_fusion) | data formatting | bytes 16777216 | tf_op jit(solution)/shard_map/convert_element_type | solution.py:54
  255.7 12.0 %all-to-all-start = ((bf16[64,32,2048]{2,1,0:T(8,128)(2,1)}), bf16[64,32,2048]{2,1,0:T(8,128)(2,1)}, u32[]{:S(2)}, u32[]{:S(2)}) async-start(bf16[64,32,2048]{2,1,0:T(8,128)(2,1)} %bitcast.80), calls=%async_computation | async-start | bytes 16777216 | tf_op jit(solution)/shard_map/all_to_all | solution.py:55
  267.8 0.2 fusion.41
  267.9 0.0 copy-done.4
  267.9 0.1 fusion.42
  268.0 0.1 compare_convert_fusion
  268.1 2.1 multiply_reduce_fusion
  270.2 0.0 copy-done.2
  270.2 3.1 fusion.49
  273.3 364.2 %all-to-all-done = bf16[64,32,2048]{2,1,0:T(8,128)(2,1)} async-done(((bf16[64,32,2048]{2,1,0:T(8,128)(2,1)}), bf16[64,32,2048]{2,1,0:T(8,128)(2,1)}, u32[]{:S(2)}, u32[]{:S(2)}) %all-to-all-start) | async-done | bytes 8388640 | tf_op jit(solution)/shard_map/all_to_all | solution.py:55
  637.5 7.1 %convolution_bitcast_fusion = f32[256,2048]{1,0:T(8,128)S(1)} fusion(bf16[64,32,2048]{2,1,0:T(8,128)(2,1)} %all-to-all-done, f32[256,64,32]{0,2,1:T(8,128)} %multiply_reduce_fusion), kind=kOutput, calls=%fused_computation.18 | convolution fusion | flops 2149580800 | bytes 12582912 | tf_op jit(solution)/shard_map/tec,ecd->td/dot_general | solution.py:108
  644.6 0.0 copy-done.1
  644.7 7.1 %fusion.11 = f32[256,2048]{1,0:T(8,128)} fusion(f32[256,2048]{1,0:T(8,128)S(1)} %convolution_bitcast_fusion, bf16[64,32,2048]{2,1,0:T(8,128)(2,1)} %all-to-all-done, f32[256,64,32]{0,2,1:T(8,128)S(1)} %copy-done.1), kind=kOutput, calls=%fused_computation.22 | convolution fusion | flops 2148532224 | bytes 14680064 | tf_op jit(solution)/shard_map/tec,ecd->td/dot_general | solution.py:107
  651.8 0.0 copy-done
  651.8 4.7 fusion.12
  (12 shorter events, 0.2 us)
Async XLA Ops:
  6.5 645.2 %copy-start = (bf16[512,2048]{1,0:T(8,128)(2,1)S(1)}, bf16[512,2048]{1,0:T(8,128)(2,1)}, u32[]{:S(2)}) copy-start(bf16[512,2048]{1,0:T(8,128)(2,1)} %param.19) | copy-start | bytes 6291460
  6.6 5.9 copy-start.3
  6.6 197.5 %all-gather.3.cloned.1.call-start = ((), (), s32[]{:S(2)}) async-start(), calls=%async_computation.1 | async-start | bytes 34603008 | tf_op jit(solution)/shard_map/all_gather | solution.py:82
  255.7 12.2 %copy-start.4 = (f32[256,4]{0,1:T(4,128)S(1)}, f32[256,4]{0,1:T(4,128)}, u32[]{:S(2)}) copy-start(f32[256,4]{0,1:T(4,128)} %param.13) | copy-start | bytes 12292
  255.7 14.5 %copy-start.2 = (bf16[256,2048]{1,0:T(8,128)(2,1)S(1)}, bf16[256,2048]{1,0:T(8,128)(2,1)}, u32[]{:S(2)}) copy-start(bf16[256,2048]{1,0:T(8,128)(2,1)} %fusion.25) | copy-start | bytes 3145732
  255.7 381.8 %all-to-all-start = ((bf16[64,32,2048]{2,1,0:T(8,128)(2,1)}), bf16[64,32,2048]{2,1,0:T(8,128)(2,1)}, u32[]{:S(2)}, u32[]{:S(2)}) async-start(bf16[64,32,2048]{2,1,0:T(8,128)(2,1)} %bitcast.80), calls=%async_computation | async-start | bytes 16777216 | tf_op jit(solution)/shard_map/all_to_all | solution.py:55
  637.5 7.1 %copy-start.1 = (f32[256,64,32]{0,2,1:T(8,128)S(1)}, f32[256,64,32]{0,2,1:T(8,128)}, u32[]{:S(2)}) copy-start(f32[256,64,32]{0,2,1:T(8,128)} %multiply_reduce_fusion) | copy-start | bytes 6291460
Sparse Core Ops, SparseCore 0:
  12.6 191.4 all-gather.2
where the time goes:
time: 664 us; the launch traced here: 663 us
  waiting for transfers between devices  516 us (78%)
  matrix products  65.8 us (10%)
  blocking collectives  39.3 us (6%)
  between operations  13.5 us (2%)
  starting transfers between devices  12 us (2%)
  local copies, waits for them, and re-layouts  8.52 us (1%)
  other arithmetic  8.16 us (1%)
    all_to_all x1, waiting for transfers between devices, serve_rows(): lax.all_to_all(produced.reshape(received.shape), EP, split_axis=0, concat...  364 us
    all_gather x1, waiting for transfers between devices, on_device(): all_normed = lax.all_gather(normed, EP, axis=0, tiled=True)  152 us
    all_gather x2, blocking collectives, stacked_from(): tiles = lax.all_gather(tiles, axes[k], axis=0, tiled=True)  39.3 us
    dot_general x1, matrix products, on_device(): jnp.einsum('ptxc,ptd->pxcd', placing_here, sources, preferred_element_typ...  17.1 us
    dot_general x1, matrix products, serve_rows(): jnp.einsum('sxch,xhd->sxcd', hidden, w_down, preferred_element_type=jnp.f...  15.3 us
  transfers between devices with their start and end apart: 2, of which 2 were waited for; matrix products, arithmetic and copies ran while one was open for 1% of the time, Pallas kernels for 0%

commit v1 on v0

v1 whole, which is shorter than its diff:
```python
import jax
import jax.numpy as jnp
from jax import lax
from jax.sharding import Mesh
from jax.sharding import PartitionSpec as P

EP = ("ep_0", "ep_1")
GRP_EP = ("grp", "ep_0", "ep_1")
CHUNKS = 2


def layer_norm(stream, norm_gain):
    widened = stream.astype(jnp.float32)
    row_mean = jnp.mean(widened, axis=-1, keepdims=True)
    variance = jnp.mean(jnp.square(widened - row_mean), axis=-1, keepdims=True)
    return ((widened - row_mean) * lax.rsqrt(variance + 1e-05) * norm_gain).astype(jnp.bfloat16)


def shared_branch(normed, shared_gate, shared_up, shared_down):
    shared_hidden = (
        jax.nn.silu(jnp.dot(normed, shared_gate, preferred_element_type=jnp.float32))
        * jnp.dot(normed, shared_up, preferred_element_type=jnp.float32)
    ).astype(jnp.bfloat16)
    return jnp.dot(shared_hidden, shared_down, preferred_element_type=jnp.float32)


def served(sources, placing, slot_gates, w_gate, w_up, w_down):
    peers, rows, width = sources.shape
    local, cap = placing.shape[2], placing.shape[3]
    incoming = jnp.einsum(
        "ptxc,ptd->xpcd", placing, sources, preferred_element_type=jnp.float32
    ).astype(jnp.bfloat16).reshape(local, peers * cap, width)
    gate_act = jnp.einsum("xnd,xdh->xnh", incoming, w_gate, preferred_element_type=jnp.float32)
    up_act = jnp.einsum("xnd,xdh->xnh", incoming, w_up, preferred_element_type=jnp.float32)
    weight = slot_gates.reshape(local, peers * cap, 1)
    hidden = (jax.nn.silu(gate_act) * up_act * weight).astype(jnp.bfloat16)
    produced = jnp.einsum(
        "xnh,xhd->xnd", hidden, w_down, preferred_element_type=jnp.float32
    ).astype(jnp.bfloat16).reshape(local, peers, cap, width)
    return jnp.einsum(
        "ptxc,xpcd->ptd", placing, produced, preferred_element_type=jnp.float32
    ).astype(jnp.bfloat16)


def on_device(
    stream, norm_gain, routing, gates, w_gate, w_up, w_down, shared_gate, shared_up, shared_down
):
    tok_rows, top_count = routing.shape
    width = stream.shape[1]
    local_count = w_gate.shape[0]
    peer_count = lax.axis_size(EP)
    experts = local_count * peer_count
    capacity = 2 * tok_rows * top_count // experts
    part = tok_rows // CHUNKS
    normed = layer_norm(stream, norm_gain)
    gathered = [
        lax.all_gather(normed[i * part : (i + 1) * part], EP, axis=0, tiled=True)
        for i in range(CHUNKS)
    ]
    tags = jnp.concatenate([routing.T.astype(jnp.float32), gates.T], axis=0)
    all_tags = lax.all_gather(tags, EP, axis=0, tiled=False)
    ids, values = all_tags[:, :top_count], all_tags[:, top_count:]
    first_expert = (lax.axis_index(EP) * local_count).astype(jnp.float32)
    mine = first_expert + jnp.arange(local_count, dtype=jnp.int32).astype(jnp.float32)
    matches = (ids[:, :, :, None] == mine).astype(jnp.float32)
    hits = jnp.sum(matches, axis=1)
    weights = jnp.sum(matches * values[:, :, :, None], axis=1)
    row_ids = jnp.arange(part, dtype=jnp.int32)
    lower = (row_ids[:, None] > row_ids[None, :]).astype(jnp.bfloat16)
    slot_ids = jnp.arange(capacity, dtype=jnp.int32).astype(jnp.float32)
    returned = []
    for i in range(CHUNKS):
        chunk_hits = hits[:, i * part : (i + 1) * part]
        chunk_weights = weights[:, i * part : (i + 1) * part]
        prior = jnp.einsum(
            "ab,pbx->pax", lower, chunk_hits.astype(jnp.bfloat16), preferred_element_type=jnp.float32
        )
        placed = chunk_hits[:, :, :, None] * (prior[:, :, :, None] == slot_ids).astype(jnp.float32)
        slot_gates = jnp.sum(placed * chunk_weights[:, :, :, None], axis=1)
        sums = served(
            gathered[i].reshape(peer_count, part, width),
            placed.astype(jnp.bfloat16),
            slot_gates.transpose(1, 0, 2),
            w_gate,
            w_up,
            w_down,
        )
        returned.append(
            lax.psum_scatter(
                sums.reshape(peer_count * part, width), EP, scatter_dimension=0, tiled=True
            )
        )
    shared = shared_branch(normed, shared_gate, shared_up, shared_down)
    routed = jnp.concatenate(returned, axis=0).astype(jnp.float32)
    return (routed + shared).astype(jnp.bfloat16)


def solution(mesh):
    torus = Mesh(mesh.devices.reshape(mesh.shape["grp"], mesh.shape["ep"] // 2, 2), ("grp", "ep_0", "ep_1"))
    return jax.shard_map(
        on_device,
        mesh=torus,
        in_specs=(
            P(GRP_EP, None),
            P(),
            P(GRP_EP, None),
            P(GRP_EP, None),
            P(EP, None, None),
            P(EP, None, None),
            P(EP, None, None),
            P(),
            P(),
            P(),
        ),
        out_specs=P(GRP_EP, None),
        check_vma=False,
    )
```

time: 664 us -> 502 us (0.76)
  waiting for transfers between devices: 516 us -> 291 us
  matrix products: 65.8 us -> 110 us
  other arithmetic: 8.16 us -> 26.3 us
  starting transfers between devices: 12 us -> 0.19 us
  local copies, waits for them, and re-layouts: 8.52 us -> 18.4 us
    all_to_all x1 -> x0, waiting for transfers between devices: 364 us -> none  [serve_rows(): lax.all_to_all(produced.reshape(received.shape), EP, split_axis=0, concat...]
    reduce_scatter x0 -> x2, waiting for transfers between devices: none -> 191 us  [on_device(): lax.psum_scatter(sums.reshape(peer_count * part, width), EP, scatter_dime...]
    all_gather x1 -> x2, waiting for transfers between devices: 152 us -> 98.4 us  [on_device(): lax.all_gather(normed[i * part:(i + 1) * part], EP, axis=0, tiled=True)]
    unnamed x0 -> x2, matrix products: none -> 28 us
    convert_element_type x1 -> x4, other arithmetic: 0.08 us -> 20.4 us  [the longest x2 19 us: served(): incoming = jnp.einsum('ptxc,ptd->xpcd', placing, sources, preferred_eleme...]
    dot_general x7 -> x8, matrix products: 58 us -> 74.9 us  [the longest x2 30.9 us: served(): jnp.einsum('xnh,xhd->xnd', hidden, w_down, preferred_element_type=jnp.flo...]
    all_to_all x1 -> x0, starting transfers between devices: 12 us -> none  [serve_rows(): lax.all_to_all(produced.reshape(received.shape), EP, split_axis=0, concat...]
    convert_element_type x2, local copies, waits for them, and re-layouts: 8.29 us -> 16.8 us  [served(): incoming = jnp.einsum('ptxc,ptd->xpcd', placing, sources, preferred_eleme...]
  transfers between devices with their start and end apart: 2 -> 4, of which waited for: 2 -> 4; matrix products, arithmetic and copies ran while one was open for 1% -> 29% of each run, Pallas kernels for 0% -> 0%
where the time goes in v1:
time: 502 us; the launch traced here: 498 us
  waiting for transfers between devices  291 us (58%)
  matrix products  110 us (22%)
  blocking collectives  38.6 us (8%)
  other arithmetic  26.3 us (5%)
  local copies, waits for them, and re-layouts  18.4 us (4%)
  between operations  13.3 us (3%)
    reduce_scatter x2, waiting for transfers between devices, on_device(): lax.psum_scatter(sums.reshape(peer_count * part, width), EP, scatter_dime...  191 us
    all_gather x2, waiting for transfers between devices, on_device(): lax.all_gather(normed[i * part:(i + 1) * part], EP, axis=0, tiled=True)  98.4 us
    all_gather x1, blocking collectives, on_device(): all_tags = lax.all_gather(tags, EP, axis=0, tiled=False)  38.6 us
    dot_general x2, matrix products, served(): jnp.einsum('xnh,xhd->xnd', hidden, w_down, preferred_element_type=jnp.flo...  30.9 us
    unnamed x2, matrix products  28 us
    dot_general x2, matrix products, served(): jnp.einsum('xnd,xdh->xnh', incoming, w_gate, preferred_element_type=jnp.f...  22.5 us
    dot_general x2, matrix products, served(): jnp.einsum('ptxc,xpcd->ptd', placing, produced, preferred_element_type=jn...  21.1 us
    convert_element_type x2, other arithmetic, served(): incoming = jnp.einsum('ptxc,ptd->xpcd', placing, sources, preferred_eleme...  19 us
  transfers between devices with their start and end apart: 4, of which 4 were waited for; matrix products, arithmetic and copies ran while one was open for 29% of the time, Pallas kernels for 0%

profile of v1, /device:TPU:196, one launch (start us, length us, event | category | flops | bytes accessed | tf_op | source)
XLA Modules:
  0.0 497.8 jit_solution(2415748811531970756)
XLA Ops:
  6.6 1.6 convert_reduce_fusion
  8.2 1.6 fusion.5
  9.8 1.6 fusion.7
  11.4 1.0 fusion.29
  12.6 0.7 all-gather.6.cloned.1.call-update
  13.5 38.6 %all-gather = f32[256,256]{1,0:T(8,128)S(1)} all-gather(f32[8,256]{1,0:T(8,128)S(1)} %pad_maximum_fusion), channel_id=2, replica_groups=mesh['grp'=4,'ep_0'=16,'ep_1'=2] {'ep_0','ep_1'}, dimensions={0}, use_global_device_ids=true | all-gather | bytes 270336 | tf_op jit(solution)/shard_map/all_gather | solution.py:61
  52.2 0.1 fusion.17
  52.5 0.1 convolution_bitcast_fusion.1
  52.7 0.1 convolution_bitcast_fusion
  52.9 0.8 fusion.9
  53.7 0.1 mul.116
  53.8 1.4 select_convert_fusion.1
  55.2 65.0 %all-gather.4.cloned.1.call-done = bf16[4096,2048]{1,0:T(8,128)(2,1)} async-done(((bf16[128,2048]{1,0:T(8,128)(2,1)}), bf16[4096,2048]{1,0:T(8,128)(2,1)}) %all-gather.4.cloned.1.call-update) | async-done | bytes 16777232 | tf_op jit(solution)/shard_map/all_gather | solution.py:57
  120.2 14.0 %fusion.36 = f32[32,2048,64]{1,2,0} fusion(bf16[32,128,64]{1,2,0:T(8,128)(2,1)} %bitcast.68, bf16[32,128,2048]{2,1,0:T(8,128)(2,1)} %bitcast.60), kind=kOutput, calls=%fused_computation.61 | convolution fusion | flops 1073741824 | bytes 34078720
  134.2 9.5 %convert_bitcast_fusion.1 = bf16[2,32,32,2048]{3,2,0,1:T(8,128)(2,1)} fusion(f32[32,2048,2,32]{1,3,2,0:T(8,128)} %bitcast.57), kind=kLoop, calls=%fused_computation.5 | loop fusion | flops 4194304 | bytes 25165824 | tf_op jit(solution)/shard_map/convert_element_type | solution.py:32
  143.7 8.4 %copy.46 = bf16[2,32,32,2048]{3,2,1,0:T(8,128)(2,1)} copy(bf16[2,32,32,2048]{3,2,0,1:T(8,128)(2,1)} %convert_bitcast_fusion.1) | data formatting | bytes 16777216 | tf_op jit(solution)/shard_map/convert_element_type | solution.py:32
  152.1 11.2 %fusion.33 = f32[2,1024,512]{2,1,0:T(8,128)} fusion(bf16[2,1024,2048]{2,1,0:T(8,128)(2,1)} %bitcast.63, bf16[2,2048,512]{2,1,0:T(8,128)(2,1)} %param.14), kind=kOutput, calls=%fused_computation.58 | convolution fusion | flops 4294967296 | bytes 16777216 | tf_op jit(solution)/shard_map/xnd,xdh->xnh/dot_general | solution.py:33
  163.3 15.5 %convolution_convert_fusion.1 = bf16[2,1024,2048]{2,1,0:T(8,128)(2,1)} fusion(bf16[2,512,2048]{2,1,0:T(8,128)(2,1)} %param.16, f32[2,1024,512]{2,1,0:T(8,128)} %fusion.33, bf16[2,1024,2048]{2,1,0:T(8,128)(2,1)} %bitcast.64, bf16[2,2048,512]{2,1,0:T(8,128)(2,1)} %param.15, f32[2,1024]{1,0:T(2,128)S(1)} %mul.116), kind=kOutput, calls=%fused_computation.7 | convolution fusion | flops 8601468928 | bytes 29368320 | tf_op jit(solution)/shard_map/xnh,xhd->xnd/dot_general | solution.py:37
  178.8 10.6 %bitcast_convert_fusion.1 = bf16[32,128,2048]{2,1,0:T(8,128)(2,1)} fusion(bf16[2,32,32,2048]{3,2,1,0:T(8,128)(2,1)} %bitcast.62, f32[32,128,2]{1,2,0:T(2,128)S(1)} %copy.45, f32[32,128,2]{1,2,0:T(2,128)S(1)} %copy.44, f32[32]{0:T(128)S(1)} %iota_convert_fusion), kind=kOutput, calls=%fused_computation.1 | convolution fusion | flops 1082654720 | bytes 25231488 | tf_op jit(solution)/shard_map/ptxc,xpcd->ptd/dot_general | solution.py:40
  189.5 0.1 reduce-scatter.5.cloned.1.call-start
  189.6 0.1 mul.125
  189.7 33.4 %all-gather.6.cloned.1.call-done = bf16[4096,2048]{1,0:T(8,128)(2,1)} async-done(((bf16[128,2048]{1,0:T(8,128)(2,1)}), bf16[4096,2048]{1,0:T(8,128)(2,1)}) %all-gather.6.cloned.1.call-update) | async-done | bytes 16777232 | tf_op jit(solution)/shard_map/all_gather | solution.py:57
  223.1 14.0 %fusion.37 = f32[32,2048,64]{1,2,0} fusion(bf16[32,128,64]{1,2,0:T(8,128)(2,1)} %bitcast.67, bf16[32,128,2048]{2,1,0:T(8,128)(2,1)} %bitcast.59), kind=kOutput, calls=%fused_computation.62 | convolution fusion | flops 1073741824 | bytes 34078720
  237.1 9.5 %convert_bitcast_fusion = bf16[2,32,32,2048]{3,2,0,1:T(8,128)(2,1)} fusion(f32[32,2048,2,32]{1,3,2,0:T(8,128)} %bitcast.58), kind=kLoop, calls=%fused_computation.4 | loop fusion | flops 4194304 | bytes 25165824 | tf_op jit(solution)/shard_map/convert_element_type | solution.py:32
  246.6 8.5 %copy.53 = bf16[2,32,32,2048]{3,2,1,0:T(8,128)(2,1)} copy(bf16[2,32,32,2048]{3,2,0,1:T(8,128)(2,1)} %convert_bitcast_fusion) | data formatting | bytes 16777216 | tf_op jit(solution)/shard_map/convert_element_type | solution.py:32
  255.1 11.3 %fusion.34 = f32[2,1024,512]{2,1,0:T(8,128)} fusion(bf16[2,1024,2048]{2,1,0:T(8,128)(2,1)} %bitcast.65, bf16[2,2048,512]{2,1,0:T(8,128)(2,1)} %param.14), kind=kOutput, calls=%fused_computation.59 | convolution fusion | flops 4294967296 | bytes 16777216 | tf_op jit(solution)/shard_map/xnd,xdh->xnh/dot_general | solution.py:33
  266.4 15.4 %convolution_convert_fusion = bf16[2,1024,2048]{2,1,0:T(8,128)(2,1)} fusion(bf16[2,512,2048]{2,1,0:T(8,128)(2,1)} %param.16, f32[2,1024,512]{2,1,0:T(8,128)} %fusion.34, bf16[2,1024,2048]{2,1,0:T(8,128)(2,1)} %bitcast.66, bf16[2,2048,512]{2,1,0:T(8,128)(2,1)} %param.15, f32[2,1024]{1,0:T(2,128)S(1)} %mul.125), kind=kOutput, calls=%fused_computation.6 | convolution fusion | flops 8601468928 | bytes 29368320 | tf_op jit(solution)/shard_map/xnh,xhd->xnd/dot_general | solution.py:37
  281.8 10.5 %bitcast_convert_fusion = bf16[32,128,2048]{2,1,0:T(8,128)(2,1)} fusion(bf16[2,32,32,2048]{3,2,1,0:T(8,128)(2,1)} %bitcast.61, f32[32,128,2]{1,2,0:T(2,128)S(1)} %copy.52, f32[32,128,2]{1,2,0:T(2,128)S(1)} %copy.51, f32[32]{0:T(128)S(1)} %iota_convert_fusion), kind=kOutput, calls=%fused_computation | convolution fusion | flops 1082654720 | bytes 25231488 | tf_op jit(solution)/shard_map/ptxc,xpcd->ptd/dot_general | solution.py:40
  292.4 3.2 fusion.35
  295.5 58.5 %reduce-scatter.3.cloned.1.call-done = bf16[128,2048]{1,0:T(8,128)(2,1)} async-done(((bf16[4096,2048]{1,0:T(8,128)(2,1)}), bf16[128,2048]{1,0:T(8,128)(2,1)}) %reduce-scatter.3.cloned.1.call-update) | async-done | bytes 524304 | tf_op jit(solution)/shard_map/reduce_scatter | solution.py:89
  354.0 132.9 %reduce-scatter.5.cloned.1.call-done = bf16[128,2048]{1,0:T(8,128)(2,1)} async-done(((bf16[4096,2048]{1,0:T(8,128)(2,1)}), bf16[128,2048]{1,0:T(8,128)(2,1)}) %reduce-scatter.5.cloned.1.call-update) | async-done | bytes 524304 | tf_op jit(solution)/shard_map/reduce_scatter | solution.py:89
  486.9 4.3 fusion.2
  (30 shorter events, 0.7 us)
Async XLA Ops:
  6.5 480.4 %copy-start = (bf16[512,2048]{1,0:T(8,128)(2,1)S(1)}, bf16[512,2048]{1,0:T(8,128)(2,1)}, u32[]{:S(2)}) copy-start(bf16[512,2048]{1,0:T(8,128)(2,1)} %param.19) | copy-start | bytes 6291460
  6.6 6.9 %copy-start.1 = (s32[256,4]{0,1:T(4,128)S(1)}, s32[256,4]{0,1:T(4,128)}, u32[]{:S(2)}) copy-start(s32[256,4]{0,1:T(4,128)} %param.12) | copy-start | bytes 12292
  6.6 6.9 %copy-start.2 = (f32[256,4]{0,1:T(4,128)S(1)}, f32[256,4]{0,1:T(4,128)}, u32[]{:S(2)}) copy-start(f32[256,4]{0,1:T(4,128)} %param.13) | copy-start | bytes 12292
  6.6 113.6 %all-gather.4.cloned.1.call-start = ((), (), s32[]{:S(2)}) async-start(), calls=%async_computation.2 | async-start | bytes 17301504 | tf_op jit(solution)/shard_map/all_gather | solution.py:57
  12.5 210.6 %all-gather.6.cloned.1.call-start = ((), (), s32[]{:S(2)}) async-start(), calls=%async_computation.4 | async-start | bytes 17301504 | tf_op jit(solution)/shard_map/all_gather | solution.py:57
  13.3 340.6 %reduce-scatter.3.cloned.1.call-start = ((), (), s32[]{:S(2)}) async-start(), calls=%async_computation.3 | async-start | bytes 17301504 | tf_op jit(solution)/shard_map/reduce_scatter | solution.py:89
  189.5 297.4 %reduce-scatter.5.cloned.1.call-start = ((), (), s32[]{:S(2)}) async-start(), calls=%async_computation.5 | async-start | bytes 17301504 | tf_op jit(solution)/shard_map/reduce_scatter | solution.py:89
Sparse Core Ops, SparseCore 0:
  12.6 107.4 all-gather.3
  121.9 101.1 all-gather.5
  225.5 128.4 reduce-scatter.2
  356.3 130.6 reduce-scatter.4
